TPU v7x, 32 devices: a whole 2x2x4 slice. The times are simulated.
32 devices in a mesh: sp: 16 (over z, y, x), tp: 2 (over core).
Axes of the slice: x: 2, y: 2, z: 4, core: 2. Of those that a mesh axis runs over, the one named last changes fastest.
Arguments:
- out_grad: bfloat16 [3584, 2048], P('sp'), may hold values from -8 to 8
- routes: int32 [3584, 2], P('sp'), may hold values from 0 to 15, all different within a row; in each aligned block of 224 rows (0 to 223, 224 to 447, ...) at most 70 rows name the same one
- route_weights: float32 [3584, 2], P('sp'), may hold values from 0.5 to 2
- routed_rows: bfloat16 [16, 16, 70, 2048], P('sp'), may hold values from -6 to 6
- gate_weight: bfloat16 [16, 2048, 1024], P('sp', None, 'tp'), may hold values from -0.125 to 0.125
- up_weight: bfloat16 [16, 2048, 1024], P('sp', None, 'tp'), may hold values from -0.125 to 0.125
- down_weight: bfloat16 [16, 1024, 2048], P('sp', 'tp'), may hold values from -0.1875 to 0.1875
- values: bfloat16 [3584, 1024], P('sp', 'tp'), may hold values from -0.625 to 0.625
- key_side: bfloat16 [3584, 512], P('sp', 'tp'), may hold values from -0.625 to 0.625
- query_side: bfloat16 [3584, 512], P('sp', 'tp'), may hold values from -0.625 to 0.625
- decay_log: float32 [16, 3584], P('tp', 'sp'), may hold values from -0.09 to 0, as said below
- gate_in: bfloat16 [3584, 1024], P('sp', 'tp'), may hold values from -6 to 6
- entry_states: float32 [16, 16, 64, 128], P('sp', 'tp'), may hold values from -6 to 6
- out_weight: bfloat16 [2048, 1024], P(None, 'tp'), may hold values from -0.1875 to 0.1875
Outputs:
- grad_hidden: bfloat16 [3584, 2048], P('sp')
- grad_gate_weight: bfloat16 [16, 2048, 1024], P('sp', None, 'tp')
- grad_up_weight: bfloat16 [16, 2048, 1024], P('sp', None, 'tp')
- grad_down_weight: bfloat16 [16, 1024, 2048], P('sp', 'tp')
- grad_out_weight: float32 [2048, 1024], P('sp', 'tp')
- grad_values: bfloat16 [3584, 1024], P('sp', 'tp')
- grad_key_side: bfloat16 [3584, 512], P('sp', 'tp')
- grad_query_side: bfloat16 [3584, 512], P('sp', 'tp')
- grad_decay: float32 [16, 3584], P('tp', 'sp')
- grad_gate_in: bfloat16 [3584, 1024], P('sp', 'tp')
Inputs may be any that keep to these rules, and one draw needn't show every extreme that they name: Each row names 2 different experts. Among the routes of one segment of 224 tokens no expert is named more than 70 times, and in some segments one expert is named exactly 70 times. `decay_log`: every entry is negative.
All inputs are finite; a program needn't handle non-finite values.
Results may differ from a plain program's by a relative error of at most 0.0072.
Values may be sent and summed in bfloat16 or wider, within the bound.
A program may use at most 128 MiB of HBM per device.

v0:
```python
import jax
import jax.numpy as jnp
from jax import lax
from jax.sharding import PartitionSpec as P

HEADS = 16
HEAD_DIM = 64
GROUPS = 4
NSTATE = 128
EXP_DEV = 1


precise = lax.Precision.HIGHEST


def entering(value, axis, join, neutral):
    count, mine = (lax.axis_size(axis), lax.axis_index(axis))
    pieces = jax.tree.map(lambda part: lax.all_gather(part, axis), value)
    pieces = jax.tree.map(lambda part: part[::-1], pieces)
    mine = count - 1 - mine
    so_far = jax.tree.map(
        lambda part, zero: jnp.full_like(part, 0) + jnp.asarray(zero, part.dtype), value, neutral
    )

    def turn(position, so_far):
        longer = join(so_far, jax.tree.map(lambda part: part[position], pieces))
        return jax.tree.map(lambda new, old: jnp.where(position < mine, new, old), longer, so_far)

    return lax.fori_loop(0, count - 1, turn, so_far)


def route_slots(routes_dev, expert_count):
    flat_routes = routes_dev.reshape(-1)
    onehot = (flat_routes[:, None] == jnp.arange(expert_count, dtype=jnp.int32)[None, :]).astype(
        jnp.int32
    )
    earlier = jnp.cumsum(onehot, axis=0) - onehot
    return jnp.sum(earlier * onehot, axis=1)


def block_forward(values, key_side, query_side, decay_log, gate_in, entry_state):
    length = values.shape[0]
    head_count = decay_log.shape[0]
    per_group = HEADS // GROUPS
    group_count = head_count // per_group
    grouped = values.reshape(length, group_count, per_group, HEAD_DIM)
    key_rows = key_side.reshape(length, group_count, NSTATE)
    query_rows = query_side.reshape(length, group_count, NSTATE)
    cumulative = jnp.cumsum(decay_log, axis=1)
    causal = jnp.tril(jnp.ones((length, length), bool))
    spread = cumulative[:, :, None] - cumulative[:, None, :]
    weights = jnp.where(causal, jnp.exp(jnp.where(causal, spread, 0.0)), 0.0)
    weights = weights.reshape(group_count, per_group, length, length)
    scores = jnp.einsum("tgn,sgn->gts", query_rows, key_rows, precision=precise)
    within = jnp.einsum("ghts,sghp->tghp", scores[:, None] * weights, grouped, precision=precise)
    carried = jnp.einsum(
        "tgn,ghpn->tghp",
        query_rows,
        entry_state.reshape(group_count, per_group, HEAD_DIM, NSTATE),
        precision=precise,
    )
    growth = jnp.exp(cumulative).reshape(group_count, per_group, length).transpose(2, 0, 1)
    core_out = (within + carried * growth[..., None]).reshape(length, head_count * HEAD_DIM)
    return core_out * jax.nn.silu(gate_in)


def end_state(values, key_side, decay_log, entry_state):
    length = values.shape[0]
    head_count = decay_log.shape[0]
    per_group = HEADS // GROUPS
    group_count = head_count // per_group
    grouped = values.reshape(length, group_count, per_group, HEAD_DIM)
    key_rows = key_side.reshape(length, group_count, NSTATE)
    cumulative = jnp.cumsum(decay_log, axis=1)
    final_sum = cumulative[:, -1]
    tail_decay = jnp.exp(final_sum[:, None] - cumulative).reshape(group_count, per_group, length)
    fresh_state = jnp.einsum("sgn,ghs,sghp->ghpn", key_rows, tail_decay, grouped, precision=precise)
    return jnp.exp(final_sum)[:, None, None] * entry_state + fresh_state.reshape(
        head_count, HEAD_DIM, NSTATE
    )


def combine(first_part, second_part):
    return (
        first_part[0] * second_part[0],
        second_part[1] + second_part[0][:, None, None] * first_part[1],
    )


def per_device(
    out_grad,
    routes,
    route_weights,
    routed_rows,
    gate_weight,
    up_weight,
    down_weight,
    values,
    key_side,
    query_side,
    decay_log,
    gate_in,
    entry_states,
    out_weight,
):
    devices = lax.axis_size("sp")
    tok_count = out_grad.shape[0]
    model_width = out_grad.shape[1]
    top_count = routes.shape[1]
    capacity = routed_rows.shape[2]
    experts = EXP_DEV * devices
    half_width = model_width // lax.axis_size("tp")
    slot_index = route_slots(routes, experts)
    target = routes.reshape(-1) * capacity + slot_index
    cot_rows = (route_weights[:, :, None] * out_grad.astype(jnp.float32)[:, None, :]).astype(
        jnp.bfloat16
    )
    outgoing = (
        jnp.zeros((experts * capacity, model_width), jnp.bfloat16)
        .at[target]
        .set(cot_rows.reshape(-1, model_width))
        .reshape(devices, EXP_DEV * capacity, model_width)
    )
    arrived = lax.all_to_all(outgoing, "sp", split_axis=0, concat_axis=0, tiled=True)
    arrived = arrived.reshape(devices, EXP_DEV, capacity, model_width)
    gate_pre = jnp.einsum(
        "escd,edf->escf", routed_rows, gate_weight, preferred_element_type=jnp.float32
    )
    up_pre = jnp.einsum(
        "escd,edf->escf", routed_rows, up_weight, preferred_element_type=jnp.float32
    )
    act = (jax.nn.silu(gate_pre) * up_pre).astype(jnp.bfloat16)
    act_grad = jnp.einsum(
        "secd,efd->escf", arrived, down_weight, preferred_element_type=jnp.float32
    )
    gate_sigmoid = jax.nn.sigmoid(gate_pre)
    gate_grad = (act_grad * up_pre * gate_sigmoid * (1.0 + gate_pre * (1.0 - gate_sigmoid))).astype(
        jnp.bfloat16
    )
    up_grad = (act_grad * jax.nn.silu(gate_pre)).astype(jnp.bfloat16)
    span_terms = jnp.einsum(
        "escf,edf->secd", gate_grad, gate_weight, preferred_element_type=jnp.float32
    )
    span_terms = span_terms + jnp.einsum(
        "escf,edf->secd", up_grad, up_weight, preferred_element_type=jnp.float32
    )
    span_terms = lax.optimization_barrier(span_terms.astype(jnp.bfloat16)).astype(jnp.float32)
    span_terms = span_terms.reshape(devices, EXP_DEV * capacity, model_width)
    grad_down_weight = jnp.einsum(
        "escf,secd->efd", act, arrived, preferred_element_type=jnp.float32
    ).astype(jnp.bfloat16)
    grad_gate_weight = jnp.einsum(
        "escd,escf->edf", routed_rows, gate_grad, preferred_element_type=jnp.float32
    ).astype(jnp.bfloat16)
    grad_up_weight = jnp.einsum(
        "escd,escf->edf", routed_rows, up_grad, preferred_element_type=jnp.float32
    ).astype(jnp.bfloat16)
    half_back = lax.psum_scatter(
        span_terms.astype(jnp.bfloat16), "tp", scatter_dimension=2, tiled=True
    )
    returned = lax.all_to_all(half_back, "sp", split_axis=0, concat_axis=0, tiled=True)
    picked = returned.reshape(experts * capacity, half_width)[target].astype(jnp.float32)
    picked = picked.reshape(tok_count, top_count, half_width).sum(axis=1)
    own_columns = lax.dynamic_slice_in_dim(
        out_grad, lax.axis_index("tp") * half_width, half_width, 1
    )
    hidden_half = (own_columns.astype(jnp.float32) + picked).astype(jnp.bfloat16)
    grad_hidden = lax.all_gather(hidden_half, "tp", axis=1, tiled=True)
    mix_cot = jnp.dot(grad_hidden, out_weight, preferred_element_type=jnp.float32)
    value_float = values.astype(jnp.float32)
    key_float = key_side.astype(jnp.float32)
    query_float = query_side.astype(jnp.float32)
    gate_float = gate_in.astype(jnp.float32)
    entry_state = entry_states[0]
    mixed_out, pull_mixed = jax.vjp(
        block_forward, value_float, key_float, query_float, decay_log, gate_float, entry_state
    )
    mixer_out = mixed_out.astype(jnp.bfloat16)
    first_grads = pull_mixed(mix_cot)
    grad_out_weight = lax.psum_scatter(
        lax.dot_general(
            grad_hidden, mixer_out, (((0,), (0,)), ((), ())), preferred_element_type=jnp.float32
        ),
        "sp",
        scatter_dimension=0,
        tiled=True,
    )
    totals = jnp.exp(jnp.sum(decay_log, axis=1))
    scanned = entering(
        (totals, first_grads[5]),
        "sp",
        combine,
        (jnp.ones_like(totals), jnp.zeros_like(first_grads[5])),
    )
    state_cot = scanned[1]
    _, pull_end = jax.vjp(end_state, value_float, key_float, decay_log, entry_state)
    second_grads = pull_end(state_cot)
    grad_values = (first_grads[0] + second_grads[0]).astype(jnp.bfloat16)
    grad_key_side = (first_grads[1] + second_grads[1]).astype(jnp.bfloat16)
    grad_query_side = first_grads[2].astype(jnp.bfloat16)
    grad_decay = first_grads[3] + second_grads[2]
    grad_gate_in = first_grads[4].astype(jnp.bfloat16)
    return (
        grad_hidden,
        grad_gate_weight,
        grad_up_weight,
        grad_down_weight,
        grad_out_weight,
        grad_values,
        grad_key_side,
        grad_query_side,
        grad_decay,
        grad_gate_in,
    )


def solution(mesh):
    in_specs = (
        P("sp", None),
        P("sp", None),
        P("sp", None),
        P("sp", None, None, None),
        P("sp", None, "tp"),
        P("sp", None, "tp"),
        P("sp", "tp", None),
        P("sp", "tp"),
        P("sp", "tp"),
        P("sp", "tp"),
        P("tp", "sp"),
        P("sp", "tp"),
        P("sp", "tp", None, None),
        P(None, "tp"),
    )
    out_specs = (
        P("sp", None),
        P("sp", None, "tp"),
        P("sp", None, "tp"),
        P("sp", "tp", None),
        P("sp", "tp"),
        P("sp", "tp"),
        P("sp", "tp"),
        P("sp", "tp"),
        P("tp", "sp"),
        P("sp", "tp"),
    )
    return jax.shard_map(
        per_device, mesh=mesh, in_specs=in_specs, out_specs=out_specs, check_vma=False
    )
```

profile of v0, /device:TPU:0, one launch (start us, length us, event | category | flops | bytes accessed | tf_op | source)
XLA Modules:
  0.0 438.6 jit_solution(190986318032160578)
XLA Ops:
  10.2 1.2 reduce-window.26
  11.8 4.8 %mul.182 = f32[224,2,2048]{2,1,0:T(2,128)} broadcast(bf16[224,2048]{1,0:T(8,128)(2,1)} %param.16), dimensions={0,2} | broadcast | bytes 4587520 | tf_op jit(solution)/shard_map/mul | solution.py:115
  16.6 5.5 %mul.183 = f32[448,2048]{1,0:T(8,128)} reshape(f32[224,2,2048]{2,1,0:T(2,128)} %mul.182) | data formatting | bytes 7340032 | tf_op jit(solution)/shard_map/mul | solution.py:115
  22.1 7.6 %scatter_custom_fusion = bf16[1120,2048]{1,0:T(8,128)(2,1)} fusion(s32[448]{0:T(512)S(1)} %bitcast.222, bf16[]{:T(256)} %constant.67.clone.1, f32[448,2048]{1,0:T(8,128)} %mul.183, f32[448]{0:T(512)S(1)} %mul.180), kind=kCustom, calls=%fused_computation.25 | custom fusion | flops 1835008 | bytes 8259586 | tf_op jit(solution)/shard_map/scatter | solution.py:121
  29.7 5.5 %reshape.270 = bf16[16,70,2048]{2,1,0:T(8,128)(2,1)} reshape(bf16[1120,2048]{1,0:T(8,128)(2,1)} %scatter_custom_fusion) | data formatting | bytes 9175040 | tf_op jit(solution)/shard_map/reshape | solution.py:122
  35.2 8.4 %all-to-all-start = ((bf16[16,70,2048]{2,1,0:T(8,128)(2,1)}), bf16[16,70,2048]{2,1,0:T(8,128)(2,1)}, u32[]{:S(2)}, u32[]{:S(2)}) async-start(bf16[16,70,2048]{2,1,0:T(8,128)(2,1)} %reshape.270), calls=%async_computation | async-start | bytes 9437184 | tf_op jit(solution)/shard_map/all_to_all | solution.py:124
  44.2 7.2 %fusion.4 = f32[16,70,512]{2,1,0:T(8,128)} fusion(bf16[16,70,2048]{2,0,1:T(8,128)(2,1)} %bitcast.227, bf16[1,2048,512]{2,1,0:T(8,128)(2,1)S(1)} %copy-done), kind=kOutput, calls=%fused_computation.13 | convolution fusion | flops 2348810240 | bytes 8978432 | tf_op jit(solution)/shard_map/escd,edf->escf/dot_general | solution.py:126
  51.4 7.3 %fusion.6 = f32[16,70,512]{2,1,0:T(8,128)} fusion(bf16[16,70,2048]{2,0,1:T(8,128)(2,1)} %bitcast.228, bf16[1,2048,512]{2,1,0:T(8,128)(2,1)S(1)} %copy-done.30), kind=kOutput, calls=%fused_computation.15 | convolution fusion | flops 2348810240 | bytes 8978432 | tf_op jit(solution)/shard_map/escd,edf->escf/dot_general | solution.py:129
  58.7 74.2 %all-to-all-done = bf16[16,70,2048]{2,1,0:T(8,128)(2,1)} async-done(((bf16[16,70,2048]{2,1,0:T(8,128)(2,1)}), bf16[16,70,2048]{2,1,0:T(8,128)(2,1)}, u32[]{:S(2)}, u32[]{:S(2)}) %all-to-all-start) | async-done | bytes 4587552 | tf_op jit(solution)/shard_map/all_to_all | solution.py:124
  132.9 7.7 %multiply_convert_fusion.2 = (bf16[16,70,512]{2,1,0:T(8,128)(2,1)S(1)}, bf16[16,70,512]{2,1,0:T(8,128)(2,1)S(1)}) fusion(f32[16,70,512]{2,1,0:T(8,128)} %fusion.4, f32[16,70,512]{2,1,0:T(8,128)} %fusion.6, bf16[16,70,2048]{2,1,0:T(8,128)(2,1)} %all-to-all-done, bf16[1,512,2048]{2,1,0:T(8,128)(2,1)} %param.22), kind=kOutput, calls=%fused_computation.21 | convolution fusion | flops 2356264960 | bytes 13565952 | tf_op jit(solution)/shard_map/secd,efd->escf/dot_general | solution.py:133
  140.6 2.7 fusion.18
  143.3 4.6 %fusion.1 = bf16[16,1,70,2048]{3,2,0,1:T(8,128)(2,1)} fusion(f32[16,70,2048]{2,1,0:T(8,128)S(1)} %fusion.18, bf16[16,70,512]{2,1,0:T(8,128)(2,1)S(1)} %get-tuple-element.178, bf16[1,2048,512]{2,1,0:T(8,128)(2,1)S(1)} %copy-done.31), kind=kOutput, calls=%fused_computation.6 | convolution fusion | flops 2353397760 | bytes 17006592 | tf_op jit(solution)/shard_map/escf,edf->secd/dot_general | solution.py:144
  148.0 29.2 %reduce-scatter.3.cloned.1.call-done = bf16[16,70,1024]{2,1,0:T(8,128)(2,1)} async-done(((bf16[16,70,2048]{2,1,0:T(8,128)(2,1)}), bf16[16,70,1024]{2,1,0:T(8,128)(2,1)}) %reduce-scatter.3.cloned.1.call-update) | async-done | bytes 2293776 | tf_op jit(solution)/shard_map/reduce_scatter | solution.py:158
  177.2 6.9 %all-to-all-start.1 = ((bf16[16,70,1024]{2,1,0:T(8,128)(2,1)}), bf16[16,70,1024]{2,1,0:T(8,128)(2,1)}, u32[]{:S(2)}, u32[]{:S(2)}) async-start(bf16[16,70,1024]{2,1,0:T(8,128)(2,1)} %reduce-scatter.3.cloned.1.call-done), calls=%async_computation.2 | async-start | bytes 4718592 | tf_op jit(solution)/shard_map/all_to_all | solution.py:161
  186.0 1.6 fusion.41
  188.7 43.1 %all-to-all-done.1 = bf16[16,70,1024]{2,1,0:T(8,128)(2,1)} async-done(((bf16[16,70,1024]{2,1,0:T(8,128)(2,1)}), bf16[16,70,1024]{2,1,0:T(8,128)(2,1)}, u32[]{:S(2)}, u32[]{:S(2)}) %all-to-all-start.1) | async-done | bytes 2293792 | tf_op jit(solution)/shard_map/all_to_all | solution.py:161
  231.8 2.7 reshape.275
  234.5 2.1 gather_fusion
  236.6 1.1 reshape.296
  237.7 2.2 reduce_sum.92
  239.9 1.3 add_convert_fusion.1
  241.2 2.5 all_gather.10
  243.7 1.4 fusion.75
  245.4 1.1 fusion.66
  248.1 47.1 %all-reduce.5 = f32[128]{0:T(128)S(1)} all-reduce(f32[128]{0:T(128)S(1)} %exponential_dynamic-update-slice_fusion), channel_id=2, replica_groups=mesh['sp'=16,'tp'=2] {'sp'}, use_global_device_ids=true, to_apply=%add.5 | all-reduce | flops 128 | bytes 1024
  296.7 10.6 %fusion.11 = bf16[1,2048,512]{1,2,0:T(8,128)(2,1)} fusion(bf16[16,70,512]{2,1,0:T(8,128)(2,1)} %copy-done.34, bf16[16,70,2048]{2,0,1:T(8,128)(2,1)} %bitcast.229), kind=kOutput, calls=%fused_computation.18 | convolution fusion | flops 2349858816 | bytes 7831552 | tf_op jit(solution)/shard_map/escd,escf->edf/dot_general | solution.py:155
  307.2 3.9 copy.131
  311.1 10.6 %fusion.8 = bf16[1,2048,512]{1,2,0:T(8,128)(2,1)} fusion(bf16[16,70,512]{2,1,0:T(8,128)(2,1)} %copy-done.35, bf16[16,70,2048]{2,0,1:T(8,128)(2,1)} %bitcast.230), kind=kOutput, calls=%fused_computation.17 | convolution fusion | flops 2349858816 | bytes 7831552 | tf_op jit(solution)/shard_map/escd,escf->edf/dot_general | solution.py:152
  321.7 4.3 copy.130
  326.0 8.2 %fusion.14 = bf16[1,512,2048]{2,1,0:T(8,128)(2,1)} fusion(bf16[16,70,2048]{2,1,0:T(8,128)(2,1)} %all-to-all-done, f32[16,70,512]{2,1,0:T(8,128)} %fusion.6, f32[16,70,512]{2,1,0:T(8,128)} %fusion.4), kind=kOutput, calls=%fused_computation.19 | convolution fusion | flops 2353299456 | bytes 11272192 | tf_op jit(solution)/shard_map/escf,secd->efd/dot_general | solution.py:149
  334.2 2.6 fusion.53
  336.9 2.8 fusion.81
  343.5 4.8 %rev.6 = f32[16,8,64,128]{3,2,1,0:T(8,128)} reverse(f32[16,8,64,128]{3,2,1,0:T(8,128)} %all-gather.3.cloned.1.call-done), dimensions={0} | reverse | bytes 8388608 | tf_op jit(solution)/shard_map/rev | solution.py:19
  348.3 26.6 %while.14 = (s32[]{:T(128)}, f32[8,64,128]{2,1,0:T(8,128)S(1)}, s32[]{:T(128)}, f32[16,8,64,128]{3,2,1,0:T(8,128)}, f32[16,8]{1,0:T(8,128)}, /*index=5*/s32[]{:T(128)}, s32[]{:T(128)}) while((s32[]{:T(128)}, f32[8,64,128]{2,1,0:T(8,128)S(1)}, s32[]{:T(128)}, f32[16,8,64,128]{3,2,1,0:T(8,128)}, f32[16,8]{1,0:T(8,128)}, ...), condition=%wide.region_11.12_spmd.clone, body=%wide.region_10.11_spmd.clone.sunk | while | flops 262148 | bytes 786641 | solution.py:29
  350.8 1.1 fusion.125
  365.0 1.1 fusion.125
  370.3 1.1 fusion.125
  372.1 1.1 fusion.125
  377.7 2.4 fusion.44
  380.1 1.9 copy.132
  383.6 2.5 reduce-window.36
  386.8 1.3 pad_bitcast_fusion.1
  388.1 3.3 reduce-window.34
  392.0 1.3 reduce-window.35
  394.0 1.7 convolution_bitcast_fusion.3
  395.7 1.7 fusion.51
  398.7 1.6 copy_bitcast_fusion
  400.3 30.6 %reduce-scatter.5.cloned.1.call-done = f32[128,512]{1,0:T(8,128)} async-done(((f32[2048,512]{1,0:T(8,128)}), f32[128,512]{1,0:T(8,128)}) %reduce-scatter.5.cloned.1.call-update) | async-done | bytes 262160 | tf_op jit(solution)/shard_map/reduce_scatter | solution.py:180
  (171 shorter events, 43.9 us)
Async XLA Ops:
  7.2 37.0 %copy-start = (bf16[1,2048,512]{2,1,0:T(8,128)(2,1)S(1)}, bf16[1,2048,512]{2,1,0:T(8,128)(2,1)}, u32[]{:S(2)}) copy-start(bf16[1,2048,512]{2,1,0:T(8,128)(2,1)} %param.20) | copy-start | bytes 6291460
  35.2 97.7 %all-to-all-start = ((bf16[16,70,2048]{2,1,0:T(8,128)(2,1)}), bf16[16,70,2048]{2,1,0:T(8,128)(2,1)}, u32[]{:S(2)}, u32[]{:S(2)}) async-start(bf16[16,70,2048]{2,1,0:T(8,128)(2,1)} %reshape.270), calls=%async_computation | async-start | bytes 9437184 | tf_op jit(solution)/shard_map/all_to_all | solution.py:124
  43.6 133.6 %reduce-scatter.3.cloned.1.call-start = ((), (), s32[]{:S(2)}) async-start(), calls=%async_computation.4 | async-start | bytes 7077888 | tf_op jit(solution)/shard_map/reduce_scatter | solution.py:158
  44.2 7.3 %copy-start.30 = (bf16[1,2048,512]{2,1,0:T(8,128)(2,1)S(1)}, bf16[1,2048,512]{2,1,0:T(8,128)(2,1)}, u32[]{:S(2)}) copy-start(bf16[1,2048,512]{2,1,0:T(8,128)(2,1)} %param.21) | copy-start | bytes 6291460
  140.6 2.7 copy-start.35
  140.6 2.7 copy-start.34
  140.6 2.7 copy-start.31
  147.9 36.3 %copy-start.25 = (f32[8,224]{1,0:T(8,128)S(1)}, f32[8,224]{1,0:T(8,128)}, u32[]{:S(2)}) copy-start(f32[8,224]{1,0:T(8,128)} %param.26) | copy-start | bytes 21508
  147.9 37.2 %copy-start.14 = (bf16[224,256]{1,0:T(8,128)(2,1)S(1)}, bf16[224,256]{1,0:T(8,128)(2,1)}, u32[]{:S(2)}) copy-start(bf16[224,256]{1,0:T(8,128)(2,1)} %param.25) | copy-start | bytes 344068
  147.9 37.2 %copy-start.18 = (bf16[224,512]{1,0:T(8,128)(2,1)S(1)}, bf16[224,512]{1,0:T(8,128)(2,1)}, u32[]{:S(2)}) copy-start(bf16[224,512]{1,0:T(8,128)(2,1)} %param.23) | copy-start | bytes 688132
  147.9 37.4 %copy-start.12 = (bf16[224,256]{1,0:T(8,128)(2,1)S(1)}, bf16[224,256]{1,0:T(8,128)(2,1)}, u32[]{:S(2)}) copy-start(bf16[224,256]{1,0:T(8,128)(2,1)} %param.24) | copy-start | bytes 344068
  148.0 37.7 %copy-start.2 = (f32[1,8,64,128]{3,2,1,0:T(8,128)S(1)}, f32[1,8,64,128]{3,2,1,0:T(8,128)}, u32[]{:S(2)}) copy-start(f32[1,8,64,128]{3,2,1,0:T(8,128)} %param.28) | copy-start | bytes 786436
  177.2 54.6 %all-to-all-start.1 = ((bf16[16,70,1024]{2,1,0:T(8,128)(2,1)}), bf16[16,70,1024]{2,1,0:T(8,128)(2,1)}, u32[]{:S(2)}, u32[]{:S(2)}) async-start(bf16[16,70,1024]{2,1,0:T(8,128)(2,1)} %reduce-scatter.3.cloned.1.call-done), calls=%async_computation.2 | async-start | bytes 4718592 | tf_op jit(solution)/shard_map/all_to_all | solution.py:161
  184.1 159.4 %all-gather.3.cloned.1.call-start = ((), (), s32[]{:S(2)}) async-start(), calls=%async_computation.6 | async-start | bytes 4456448 | tf_op jit(solution)/shard_map/all_gather | solution.py:18
  185.1 2.6 copy-start.27
  185.1 2.5 copy-start.10
  185.3 2.4 copy-start.3
  185.3 2.3 copy-start.22
  185.6 2.1 copy-start.15
  186.0 2.6 copy-start.6
  239.9 3.8 copy-start.9
  239.9 3.8 copy-start.19
  239.9 3.8 copy-start.32
  243.7 1.7 copy-start.11
  245.1 1.4 copy-start.26
  245.1 1.5 copy-start.13
  245.1 1.6 copy-start.33
  246.5 184.5 %reduce-scatter.5.cloned.1.call-start = ((), (), s32[]{:S(2)}) async-start(), calls=%async_computation.5 | async-start | bytes 4456448 | tf_op jit(solution)/shard_map/reduce_scatter | solution.py:180
  326.0 8.2 %copy-start.4 = (bf16[224,512]{0,1:T(8,128)(2,1)S(1)}, bf16[224,512]{0,1:T(8,128)(2,1)}, u32[]{:S(2)}) copy-start(bf16[224,512]{0,1:T(8,128)(2,1)} %copy-done.3) | copy-start | bytes 688132
  326.0 8.2 %copy-start.16 = (f32[2,224,224]{2,1,0:T(8,128)S(1)}, f32[2,224,224]{2,1,0:T(8,128)}, u32[]{:S(2)}) copy-start(f32[2,224,224]{2,1,0:T(8,128)} %copy-done.15) | copy-start | bytes 1204228
  326.0 8.2 %copy-start.23 = (pred[224,224]{1,0:T(8,128)(4,1)S(1)}, pred[224,224]{1,0:T(8,128)(4,1)}, u32[]{:S(2)}) copy-start(pred[224,224]{1,0:T(8,128)(4,1)} %copy-done.22) | copy-start | bytes 150532
  326.0 8.2 %copy-start.28 = (f32[2,4,224]{2,1,0:T(4,128)S(1)}, f32[2,4,224]{2,1,0:T(4,128)}, u32[]{:S(2)}) copy-start(f32[2,4,224]{2,1,0:T(4,128)} %copy-done.27) | copy-start | bytes 21508
  334.2 2.7 copy-start.20
  336.9 5.7 %copy-start.8 = (f32[2,224,224]{2,1,0:T(8,128)}, f32[2,224,224]{2,1,0:T(8,128)S(1)}, u32[]{:S(2)}) copy-start(f32[2,224,224]{2,1,0:T(8,128)S(1)} %get-tuple-element.165) | copy-start | bytes 1204228
  339.6 1.0 copy-start.7
  348.3 27.9 %copy-start.29 = (f32[8]{0:T(128)S(1)}, f32[8]{0:T(128)}, u32[]{:S(2)}) copy-start(f32[8]{0:T(128)} %slice_reduce_fusion.4) | copy-start | bytes 100
  348.3 29.3 %copy-start.17 = (f32[2,224,224]{2,1,0:T(8,128)S(1)}, f32[2,224,224]{2,1,0:T(8,128)}, u32[]{:S(2)}) copy-start(f32[2,224,224]{2,1,0:T(8,128)} %copy-done.15) | copy-start | bytes 1204228
  377.0 3.1 copy-start.21
  377.7 2.5 copy-start.24
  377.7 16.3 %copy-start.5 = (bf16[224,512]{0,1:T(8,128)(2,1)S(1)}, bf16[224,512]{0,1:T(8,128)(2,1)}, u32[]{:S(2)}) copy-start(bf16[224,512]{0,1:T(8,128)(2,1)} %copy-done.3) | copy-start | bytes 688132
  380.1 51.8 %copy-start.1 = (bf16[1,2048,512]{2,1,0:T(8,128)(2,1)S(1)}, bf16[1,2048,512]{2,1,0:T(8,128)(2,1)}, u32[]{:S(2)}) copy-start(bf16[1,2048,512]{2,1,0:T(8,128)(2,1)} %param.20) | copy-start | bytes 6291460
Sparse Core Ops, SparseCore 0:
  148.0 29.0 reduce-scatter.2
  246.6 81.7 all-gather.2
  339.8 91.1 reduce-scatter.4
where the time goes:
time: 447 us; the launch traced here: 439 us
  waiting for transfers between devices  177 us (40%)
  matrix products  77.2 us (17%)
  local copies, waits for them, and re-layouts  62.3 us (14%)
  blocking collectives  49.6 us (11%)
  other arithmetic  40.8 us (9%)
  starting transfers between devices  16 us (4%)
  between operations  15.3 us (3%)
    all_to_all x1, waiting for transfers between devices, per_device(): lax.all_to_all(outgoing, 'sp', split_axis=0, concat_axis=0, tiled=True)  74.2 us
    unnamed x1, blocking collectives  47.1 us
    all_to_all x1, waiting for transfers between devices, per_device(): lax.all_to_all(half_back, 'sp', split_axis=0, concat_axis=0, tiled=True)  43.1 us
    reduce_scatter x1, waiting for transfers between devices, per_device(): lax.psum_scatter(lax.dot_general(grad_hidden, mixer_out, (((0,), (0,)), (...  30.6 us
    reduce_scatter x1, waiting for transfers between devices, per_device(): lax.psum_scatter(span_terms.astype(jnp.bfloat16), 'tp', scatter_dimension...  29.2 us
    select_n x15, other arithmetic, turn(): jnp.where(position < mine, new, old)  15.7 us
    unnamed x82, local copies, waits for them, and re-layouts  14.7 us
    dot_general x1, matrix products, per_device(): jnp.einsum('escd,escf->edf', routed_rows, gate_grad, preferred_element_ty...  10.6 us
  transfers between devices with their start and end apart: 5, of which 4 were waited for; matrix products, arithmetic and copies ran while one was open for 28% of the time, Pallas kernels for 0%

commit v1 on v0

v1 whole, which is shorter than its diff:
```python
import jax
import jax.numpy as jnp
from jax import lax
from jax.sharding import PartitionSpec as P

HEADS = 16
HEAD_DIM = 64
GROUPS = 4

precise = lax.Precision.HIGHEST
f32 = jnp.float32
bf16 = jnp.bfloat16


def mm(spec, a, b):
    return jnp.einsum(spec, a, b, preferred_element_type=f32)


def swap_tp(x):
    n = lax.axis_size("tp")
    return lax.ppermute(x, "tp", [(i, (i + 1) % n) for i in range(n)])


def route_slots(routes_dev, expert_count):
    flat_routes = routes_dev.reshape(-1)
    onehot = (flat_routes[:, None] == jnp.arange(expert_count, dtype=jnp.int32)[None, :]).astype(
        jnp.int32
    )
    earlier = jnp.cumsum(onehot, axis=0) - onehot
    return jnp.sum(earlier * onehot, axis=1)


def halving(part, order):
    devices = part.shape[0]
    bits = devices.bit_length() - 1
    me = lax.axis_index("sp")
    left = list(range(bits - 1, -1, -1))
    part = part.reshape((2,) * bits + part.shape[1:])
    for bit in order:
        axis = left.index(bit)
        mine = (me >> bit) & 1
        keep = lax.dynamic_index_in_dim(part, mine, axis, keepdims=False)
        send = lax.dynamic_index_in_dim(part, 1 - mine, axis, keepdims=False).astype(bf16)
        got = lax.ppermute(send, "sp", [(i, i ^ (1 << bit)) for i in range(devices)])
        part = keep + got.astype(f32)
        left.pop(axis)
    return part


def per_device(
    out_grad,
    routes,
    route_weights,
    routed_rows,
    gate_weight,
    up_weight,
    down_weight,
    values,
    key_side,
    query_side,
    decay_log,
    gate_in,
    entry_states,
    out_weight,
):
    devices = lax.axis_size("sp")
    tp = lax.axis_index("tp")
    length, width = out_grad.shape
    half = width // lax.axis_size("tp")
    capacity = routed_rows.shape[2]
    cap = (capacity + 7) // 8 * 8
    rows = devices * cap
    gate_weight, up_weight, down_weight = gate_weight[0], up_weight[0], down_weight[0]
    hidden = gate_weight.shape[1]

    def own(x, axis):
        return lax.dynamic_slice_in_dim(x, tp * half, half, axis)

    def other(x, axis):
        return lax.dynamic_slice_in_dim(x, (1 - tp) * half, half, axis)

    target = routes * cap + route_slots(routes, devices).reshape(routes.shape)
    row_ids = jnp.arange(rows, dtype=jnp.int32)
    match = row_ids[:, None, None] == target.T[None]
    select = jnp.any(match, axis=1).astype(bf16)
    row_weight = jnp.sum(jnp.where(match, route_weights.T[None], 0.0), axis=(1, 2))
    out_half = own(out_grad, 1)
    outgoing = (mm("rt,td->rd", select, out_half) * row_weight[:, None]).astype(bf16)
    arrived = lax.all_to_all(outgoing, "sp", split_axis=0, concat_axis=0, tiled=True)

    saved = jnp.pad(routed_rows[0], ((0, 0), (0, cap - capacity), (0, 0))).reshape(rows, width)
    gate_pre = mm("rd,df->rf", saved, gate_weight)
    up_pre = mm("rd,df->rf", saved, up_weight)
    joined = jnp.concatenate([gate_weight, up_weight], axis=1)
    joined_own, joined_other = own(joined, 0), other(joined, 0)
    down_own, down_other = own(down_weight, 1), other(down_weight, 1)
    act = (jax.nn.silu(gate_pre) * up_pre).astype(bf16)

    heads = decay_log.shape[0]
    per_group = HEADS // GROUPS
    groups = heads // per_group

    def by_head(x):
        return x.reshape(length, groups, per_group, HEAD_DIM).transpose(1, 2, 0, 3)

    def by_token(x):
        return x.transpose(2, 0, 1, 3).reshape(length, heads * HEAD_DIM)

    key = key_side.reshape(length, groups, -1).transpose(1, 0, 2)
    query = query_side.reshape(length, groups, -1).transpose(1, 0, 2)
    nstate = key.shape[2]
    value = by_head(values)
    entry = entry_states[0].reshape(groups, per_group, HEAD_DIM, nstate)
    entry_b = entry.astype(bf16)
    steps = jnp.arange(length)
    causal = steps[:, None] >= steps[None, :]
    tri = causal.astype(f32)
    cum = jnp.einsum("hu,tu->ht", decay_log, tri, precision=precise)
    total = cum[:, -1]
    spread = cum[:, :, None] - cum[:, None, :]
    weights = jnp.where(causal, jnp.exp(jnp.where(causal, spread, 0.0)), 0.0)
    weights = weights.reshape(groups, per_group, length, length)
    cum4 = cum.reshape(groups, per_group, length, 1)
    growth = jnp.exp(cum4)
    tail = jnp.exp(total.reshape(groups, per_group, 1, 1) - cum4)
    scores = mm("gtn,gsn->gts", query, key)
    mix = (scores[:, None] * weights).astype(bf16)
    within = mm("grts,grsp->grtp", mix, value)
    carried = growth * mm("gtn,grpn->grtp", query, entry_b)
    gate = by_head(gate_in).astype(f32)
    sig = jax.nn.sigmoid(gate)
    silu_gate = gate * sig
    core = within + carried
    core_slope = core * (sig * (1.0 + gate * (1.0 - sig)))
    mixer_out = by_token((core * silu_gate).astype(bf16))

    arrived, gate_pre, up_pre, act, saved, mix, weights, within, carried, core_slope, mixer_out, \
        silu_gate, joined_own, joined_other, down_own, down_other, value = \
        lax.optimization_barrier((
            arrived, gate_pre, up_pre, act, saved, mix, weights, within, carried, core_slope,
            mixer_out, silu_gate, joined_own, joined_other, down_own, down_other, value))

    arrived_other = swap_tp(arrived)
    act_grad = mm("rd,fd->rf", arrived, down_own)
    act_grad = act_grad + mm("rd,fd->rf", arrived_other, down_other)
    gate_sigmoid = jax.nn.sigmoid(gate_pre)
    gate_grad = (act_grad * up_pre * gate_sigmoid * (1.0 + gate_pre * (1.0 - gate_sigmoid))).astype(bf16)
    up_grad = (act_grad * (gate_pre * gate_sigmoid)).astype(bf16)
    both = jnp.concatenate([gate_grad, up_grad], axis=1)
    give = mm("rf,df->rd", both, joined_other).astype(bf16)
    got = swap_tp(give)
    keep = mm("rf,df->rd", both, joined_own).astype(bf16)
    half_back = (keep.astype(f32) + got.astype(f32)).astype(bf16)
    returned = lax.all_to_all(half_back, "sp", split_axis=0, concat_axis=0, tiled=True)

    cot_rows = jnp.where(
        tp == 0,
        jnp.concatenate([arrived, arrived_other], axis=1),
        jnp.concatenate([arrived_other, arrived], axis=1),
    )
    grad_down = mm("rf,rd->fd", act, cot_rows).astype(bf16)
    grad_gate = mm("rd,rf->df", saved, gate_grad).astype(bf16)
    grad_up = mm("rd,rf->df", saved, up_grad).astype(bf16)
    returned, grad_down, grad_gate, grad_up = lax.optimization_barrier(
        (returned, grad_down, grad_gate, grad_up)
    )

    picked = mm("rt,rd->td", select, returned)
    hidden_half = (out_half.astype(f32) + picked).astype(bf16)
    grad_hidden = lax.all_gather(hidden_half, "tp", axis=1, tiled=True)

    mix_cot = by_head(mm("td,di->ti", grad_hidden, out_weight))
    cot = mix_cot * silu_gate
    cot_b = cot.astype(bf16)
    cot_r = cot_b.astype(f32)
    grown = (growth * cot_r).astype(bf16)
    entry_grad = mm("grtp,gtn->grpn", grown, query)

    piece = entry_grad.reshape(heads, devices, HEAD_DIM // devices * nstate).transpose(1, 0, 2)
    totals = jnp.broadcast_to(total[None, :, None], (devices, heads, 1))
    piece = jnp.concatenate([piece, totals], axis=2)
    piece = lax.all_to_all(piece, "sp", split_axis=0, concat_axis=0, tiled=True)

    share = mm("td,ti->di", grad_hidden, mixer_out)
    share, cot_b = lax.optimization_barrier((share, cot_b))
    split = share.shape[1] // 2
    blocks = share.reshape(devices, width // devices, share.shape[1])
    bits = devices.bit_length() - 1
    orders = list(range(bits)), list(range(bits))
    mid = bits // 2 - 1
    orders[1][0], orders[1][mid] = orders[1][mid], orders[1][0]
    grad_out = jnp.concatenate(
        [halving(blocks[:, :, :split], orders[0]), halving(blocks[:, :, split:], orders[1])], axis=1
    )

    piece, all_total = piece[:, :, :-1], piece[:, :, -1]
    seg = jnp.arange(devices)
    between = (seg[None, None, :] > seg[:, None, None]) & (seg[None, None, :] < seg[None, :, None])
    chain = jnp.einsum("jik,kh->hji", between.astype(f32), all_total, precision=precise)
    chain = jnp.where((seg[None, :] > seg[:, None])[None], jnp.exp(chain), 0.0)
    chained = jnp.einsum("hji,ihx->jhx", chain, piece, precision=precise)
    chained = lax.all_to_all(chained, "sp", split_axis=0, concat_axis=0, tiled=True)
    state = chained.transpose(1, 0, 2).reshape(groups, per_group, HEAD_DIM, nstate)
    state_b = state.astype(bf16)

    grad_gate_in = by_token((mix_cot * core_slope).astype(bf16))
    mix_grad = mm("grtp,grsp->grts", cot_b, value)
    score_grad = jnp.sum(mix_grad * weights, axis=1).astype(bf16)
    query_grad = mm("gts,gsn->gtn", score_grad, key) + mm("grtp,grpn->gtn", grown, entry_b)
    key_grad = mm("gts,gtn->gsn", score_grad, query)
    value_f = value.astype(f32)
    value_grad = mm("grts,grtp->grsp", mix, cot_b)
    decay_rows = jnp.sum(cot_r * within + cot * carried - value_f * value_grad, axis=3)

    value_tail = tail * mm("gsn,grpn->grsp", key, state_b)
    key_grad = key_grad + mm("grsp,grpn->gsn", (tail * value_f).astype(bf16), state_b)
    tail_rows = jnp.sum(value_f * value_tail, axis=3)
    last = jnp.exp(total) * jnp.sum(entry * state, axis=(2, 3)).reshape(heads)
    grad_decay = jnp.einsum(
        "ht,tu->hu", (decay_rows - tail_rows).reshape(heads, length), tri, precision=precise
    )
    grad_decay = grad_decay + (jnp.sum(tail_rows, axis=2).reshape(heads) + last)[:, None]
    flat = lambda x: x.transpose(1, 0, 2).reshape(length, groups * nstate).astype(bf16)
    return (
        grad_hidden,
        grad_gate[None],
        grad_up[None],
        grad_down[None],
        grad_out,
        by_token((value_grad + value_tail).astype(bf16)),
        flat(key_grad),
        flat(query_grad),
        grad_decay,
        grad_gate_in,
    )


def solution(mesh):
    in_specs = (
        P("sp", None),
        P("sp", None),
        P("sp", None),
        P("sp", None, None, None),
        P("sp", None, "tp"),
        P("sp", None, "tp"),
        P("sp", "tp", None),
        P("sp", "tp"),
        P("sp", "tp"),
        P("sp", "tp"),
        P("tp", "sp"),
        P("sp", "tp"),
        P("sp", "tp", None, None),
        P(None, "tp"),
    )
    out_specs = (
        P("sp", None),
        P("sp", None, "tp"),
        P("sp", None, "tp"),
        P("sp", "tp", None),
        P("sp", "tp"),
        P("sp", "tp"),
        P("sp", "tp"),
        P("sp", "tp"),
        P("tp", "sp"),
        P("sp", "tp"),
    )
    return jax.shard_map(
        per_device, mesh=mesh, in_specs=in_specs, out_specs=out_specs, check_vma=False
    )
```

time: 447 us -> 239 us (0.53); the launches traced: 439 us -> 238 us
  waiting for transfers between devices: 177 us -> 62.4 us
  blocking collectives: 49.6 us -> 2.85 us
  starting transfers between devices: 16 us -> 50.2 us
  local copies, waits for them, and re-layouts: 62.3 us -> 38.5 us
  other arithmetic: 40.8 us -> 21.7 us
  matrix products: 77.2 us -> 60.6 us
  between operations: 15.3 us -> 1.44 us
    reduce_scatter x2 -> x0, waiting for transfers between devices: 59.8 us -> none  [the longest x1 30.6 us: per_device(): lax.psum_scatter(lax.dot_general(grad_hidden, mixer_out, (((0,), (0,)), (...]
    all_to_all x1, waiting for transfers between devices: 74.2 us -> 15.2 us  [per_device(): lax.all_to_all(outgoing, 'sp', split_axis=0, concat_axis=0, tiled=True)]
    unnamed x1 -> x0, blocking collectives: 47.1 us -> none
    mul x21 -> x0, local copies, waits for them, and re-layouts: 21.4 us -> none  [the longest x15 10.5 us: combine(): second_part[0][:, None, None] * first_part[1]]
    ppermute x0 -> x10, waiting for transfers between devices: none -> 18.4 us  [the longest x8 12.5 us: halving(): got = lax.ppermute(send, 'sp', [(i, i ^ 1 << bit) for i in range(devices)])]
    dot_general x21 -> x28, matrix products: 77.2 us -> 60.6 us  [the longest x24 57.8 us: mm(): return jnp.einsum(spec, a, b, preferred_element_type=f32)]
    all_to_all x0 -> x2, starting transfers between devices: none -> 16.4 us  [the longest x1 11.6 us: per_device(): piece = lax.all_to_all(piece, 'sp', split_axis=0, concat_axis=0, tiled=True)]
    all_to_all x1, waiting for transfers between devices: 43.1 us -> 28.8 us  [per_device(): lax.all_to_all(half_back, 'sp', split_axis=0, concat_axis=0, tiled=True)]
  transfers between devices with their start and end apart: 5 -> 14, of which waited for: 4 -> 8; matrix products, arithmetic and copies ran while one was open for 28% -> 29% of each run, Pallas kernels for 0% -> 0%
where the time goes in v1:
time: 239 us; the launch traced here: 238 us
  waiting for transfers between devices  62.4 us (26%)
  matrix products  60.6 us (25%)
  starting transfers between devices  50.2 us (21%)
  local copies, waits for them, and re-layouts  38.5 us (16%)
  other arithmetic  21.7 us (9%)
  blocking collectives  2.85 us (1%)
    dot_general x24, matrix products, mm(): return jnp.einsum(spec, a, b, preferred_element_type=f32)  57.8 us
    all_to_all x1, waiting for transfers between devices, per_device(): lax.all_to_all(half_back, 'sp', split_axis=0, concat_axis=0, tiled=True)  28.8 us
    unnamed x111, local copies, waits for them, and re-layouts  17.2 us
    all_to_all x1, waiting for transfers between devices, per_device(): lax.all_to_all(outgoing, 'sp', split_axis=0, concat_axis=0, tiled=True)  15.2 us
    ppermute x8, starting transfers between devices, halving(): got = lax.ppermute(send, 'sp', [(i, i ^ 1 << bit) for i in range(devices)])  13.6 us
    ppermute x8, waiting for transfers between devices, halving(): got = lax.ppermute(send, 'sp', [(i, i ^ 1 << bit) for i in range(devices)])  12.5 us
    all_to_all x1, starting transfers between devices, per_device(): piece = lax.all_to_all(piece, 'sp', split_axis=0, concat_axis=0, tiled=True)  11.6 us
    all_to_all x1, starting transfers between devices, per_device(): lax.all_to_all(half_back, 'sp', split_axis=0, concat_axis=0, tiled=True)  11.3 us
  transfers between devices with their start and end apart: 14, of which 8 were waited for; matrix products, arithmetic and copies ran while one was open for 29% of the time, Pallas kernels for 0%

profile of v1, /device:TPU:0, one launch (start us, length us, event | category | flops | bytes accessed | tf_op | source)
XLA Modules:
  0.0 237.8 jit_solution(11670647285779657097)
XLA Ops:
  5.5 3.4 %fusion.7 = bf16[1152,1024]{1,0:T(8,128)(2,1)} fusion(pred[1152,224]{0,1:T(8,128)(4,1)S(1)} %fusion.11, f32[1152]{0:T(1024)S(1)} %select_reduce_fusion, bf16[224,2048]{1,0:T(8,128)(2,1)} %param.14, s32[]{:T(128)S(6)} %select_n.71), kind=kOutput, calls=%fused_computation.15 | convolution fusion | flops 530841600 | bytes 3080708 | tf_op jit(solution)/shard_map/rt,td->rd/dot_general | solution.py:16
  8.9 8.7 %all-to-all-start = ((bf16[16,72,1024]{2,1,0:T(8,128)(2,1)}), bf16[16,72,1024]{2,1,0:T(8,128)(2,1)}, u32[]{:S(2)}, u32[]{:S(2)}) async-start(bf16[16,72,1024]{2,1,0:T(8,128)(2,1)} %bitcast.266), calls=%async_computation | async-start | bytes 4718592 | tf_op jit(solution)/shard_map/all_to_all | solution.py:89
  19.2 7.0 %copy.239 = bf16[1,16,70,2048]{3,2,1,0:T(8,128)(2,1)} copy(bf16[1,16,70,2048]{3,1,2,0:T(8,128)(2,1)} %param.17) | data formatting | bytes 9175040 | tf_op args[3]
  26.1 3.1 %pad.9 = bf16[16,72,2048]{2,1,0:T(8,128)(2,1)S(1)} pad(bf16[16,70,2048]{2,1,0:T(8,128)(2,1)} %bitcast.250, bf16[]{:T(256)} %constant.80.clone.1), padding=0_0x0_2x0_0 | pad | bytes 9306114 | tf_op jit(solution)/shard_map/jit(_pad)/pad | solution.py:91
  29.3 1.6 dynamic-slice_bitcast_fusion
  31.9 1.5 copy-done.10
  34.0 2.6 %fusion.9 = (bf16[1024,1024]{1,0:T(8,128)(2,1)}, bf16[1024,1024]{1,0:T(8,128)(2,1)}) fusion(s32[]{:T(128)S(6)} %select_n.75, bf16[2048,512]{1,0:T(8,128)(2,1)S(1)} %bitcast.267, bf16[2048,512]{1,0:T(8,128)(2,1)S(1)} %bitcast.268, s32[]{:T(128)S(6)} %select_n.71), kind=kLoop, calls=%fused_computation.27 | loop fusion | flops 8388608 | bytes 8388616 | tf_op jit(solution)/shard_map/concatenate | solution.py:94
  37.7 1.4 multiply_multiply_fusion
  39.1 2.0 exponential_select_fusion
  41.1 2.6 %fusion.70 = f32[1152,512]{1,0:T(8,128)S(1)} fusion(bf16[1152,2048]{1,0:T(8,128)(2,1)S(1)} %bitcast.255, bf16[1,2048,512]{2,1,0:T(8,128)(2,1)S(1)} %copy-done.10), kind=kOutput, calls=%fused_computation.157 | convolution fusion | flops 2415919104 | bytes 9175040 | tf_op jit(solution)/shard_map/rd,df->rf/dot_general | solution.py:16
  43.7 1.4 copy-done.43
  45.1 4.8 %multiply_convert_fusion.2 = (bf16[1152,512]{1,0:T(8,128)(2,1)}, f32[1152,512]{1,0:T(8,128)}) fusion(f32[1152,512]{1,0:T(8,128)S(1)} %fusion.70, bf16[1152,2048]{1,0:T(8,128)(2,1)S(1)} %bitcast.256, bf16[1,2048,512]{2,1,0:T(8,128)(2,1)S(1)} %copy-done.11), kind=kOutput, calls=%fused_computation.26 | convolution fusion | flops 2419458048 | bytes 12713984 | tf_op jit(solution)/shard_map/rd,df->rf/dot_general | solution.py:16
  49.9 15.2 %all-to-all-done = bf16[16,72,1024]{2,1,0:T(8,128)(2,1)} async-done(((bf16[16,72,1024]{2,1,0:T(8,128)(2,1)}), bf16[16,72,1024]{2,1,0:T(8,128)(2,1)}, u32[]{:S(2)}, u32[]{:S(2)}) %all-to-all-start) | async-done | bytes 2359328 | tf_op jit(solution)/shard_map/all_to_all | solution.py:89
  65.1 3.2 %fusion.74 = f32[1152,512]{1,0:T(8,128)S(1)} fusion(bf16[1152,1024]{1,0:T(8,128)(2,1)} %bitcast.4, bf16[512,1024]{1,0:T(8,128)(2,1)S(1)} %copy-done.22), kind=kOutput, calls=%fused_computation.162 | convolution fusion | flops 1207959552 | bytes 5767168 | tf_op jit(solution)/shard_map/rd,fd->rf/dot_general | solution.py:16
  68.4 1.5 collective-permute-done
  69.8 2.6 %multiply_convert_fusion.1 = (bf16[1152,512]{1,0:T(8,128)(2,1)S(1)}, bf16[1152,512]{1,0:T(8,128)(2,1)S(1)}) fusion(f32[1152,512]{1,0:T(8,128)S(1)} %copy-done.44, f32[1152,512]{1,0:T(8,128)S(1)} %copy-done.45, f32[1152,512]{1,0:T(8,128)S(1)} %fusion.74, bf16[1152,1024]{1,0:T(8,128)(2,1)S(1)} %collective-permute-done, bf16[512,1024]{1,0:T(8,128)(2,1)S(1)} %copy-done.21), kind=kOutput, calls=%fused_computation.24 | convolution fusion | flops 1216217088 | bytes 12845056 | tf_op jit(solution)/shard_map/rd,fd->rf/dot_general | solution.py:16
  72.5 2.9 %convolution_convert_fusion = bf16[1152,1024]{1,0:T(8,128)(2,1)S(1)} fusion(bf16[1024,1024]{1,0:T(8,128)(2,1)S(1)} %copy-done.13, bf16[1152,512]{1,0:T(8,128)(2,1)S(1)} %get-tuple-element.122, bf16[1152,512]{1,0:T(8,128)(2,1)S(1)} %get-tuple-element.121), kind=kOutput, calls=%fused_computation.16 | convolution fusion | flops 2421817344 | bytes 6815744 | tf_op jit(solution)/shard_map/rf,df->rd/dot_general | solution.py:16
  75.6 4.4 %collective-permute-done.1 = bf16[1152,1024]{1,0:T(8,128)(2,1)S(1)} collective-permute-done((bf16[1152,1024]{1,0:T(8,128)(2,1)S(1)}, bf16[1152,1024]{1,0:T(8,128)(2,1)S(1)}, u32[]{:S(2)}, u32[]{:S(2)}) %collective-permute-start.1) | collective-permute-done | bytes 2359328 | tf_op jit(solution)/shard_map/ppermute | solution.py:21
  80.0 4.0 %add_convert_fusion = bf16[1152,1024]{1,0:T(8,128)(2,1)} fusion(bf16[1152,1024]{1,0:T(8,128)(2,1)S(1)} %collective-permute-done.1, bf16[1024,1024]{1,0:T(8,128)(2,1)S(1)} %copy-done.12, bf16[1152,512]{1,0:T(8,128)(2,1)S(1)} %get-tuple-element.122, bf16[1152,512]{1,0:T(8,128)(2,1)S(1)} %get-tuple-element.121), kind=kOutput, calls=%fused_computation.13 | convolution fusion | flops 2426535936 | bytes 9175040 | tf_op jit(solution)/shard_map/rf,df->rd/dot_general | solution.py:16
  84.0 11.3 %all-to-all-start.1 = ((bf16[16,72,1024]{2,1,0:T(8,128)(2,1)}), bf16[16,72,1024]{2,1,0:T(8,128)(2,1)}, u32[]{:S(2)}, u32[]{:S(2)}) async-start(bf16[16,72,1024]{2,1,0:T(8,128)(2,1)} %bitcast.265), calls=%async_computation.1 | async-start | bytes 4718592 | tf_op jit(solution)/shard_map/all_to_all | solution.py:154
  95.9 7.1 %convolution_convert_fusion.2 = bf16[2048,512]{1,0:T(8,128)(2,1)} fusion(bf16[1152,2048]{1,0:T(8,128)(2,1)} %bitcast.257, bf16[1152,512]{1,0:T(8,128)(2,1)} %copy-done.48), kind=kOutput, calls=%fused_computation.20 | convolution fusion | flops 2416967680 | bytes 7995392 | tf_op jit(solution)/shard_map/rd,rf->df/dot_general | solution.py:16
  103.0 4.1 %convolution_convert_fusion.3 = bf16[2048,512]{1,0:T(8,128)(2,1)} fusion(bf16[1152,2048]{1,0:T(8,128)(2,1)S(1)} %bitcast.260, bf16[1152,512]{1,0:T(8,128)(2,1)S(1)} %copy-done.47), kind=kOutput, calls=%fused_computation.21 | convolution fusion | flops 2416967680 | bytes 7995392 | tf_op jit(solution)/shard_map/rd,rf->df/dot_general | solution.py:16
  107.1 7.0 %fusion.8 = bf16[512,2048]{1,0:T(8,128)(2,1)} fusion(bf16[1152,512]{1,0:T(8,128)(2,1)S(1)} %copy-done.49, bf16[1152,1024]{1,0:T(8,128)(2,1)S(1)} %copy-done.40, bf16[1152,1024]{1,0:T(8,128)(2,1)} %bitcast.4, pred[]{:T(512)S(6)} %eq.48), kind=kOutput, calls=%fused_computation.19 | convolution fusion | flops 2438201344 | bytes 7995393 | tf_op jit(solution)/shard_map/rf,rd->fd/dot_general | solution.py:16
  114.1 28.8 %all-to-all-done.1 = bf16[16,72,1024]{2,1,0:T(8,128)(2,1)} async-done(((bf16[16,72,1024]{2,1,0:T(8,128)(2,1)}), bf16[16,72,1024]{2,1,0:T(8,128)(2,1)}, u32[]{:S(2)}, u32[]{:S(2)}) %all-to-all-start.1) | async-done | bytes 2359328 | tf_op jit(solution)/shard_map/all_to_all | solution.py:154
  142.9 2.4 %fusion.12 = bf16[224,1024]{1,0:T(8,128)(2,1)S(1)} fusion(pred[1152,224]{0,1:T(8,128)(4,1)S(1)} %copy-done.32, bf16[1152,1024]{1,0:T(8,128)(2,1)} %bitcast.28, bf16[224,2048]{1,0:T(8,128)(2,1)S(1)} %copy-done.41, s32[]{:T(128)S(6)} %select_n.71), kind=kOutput, calls=%fused_computation.36 | convolution fusion | flops 529170432 | bytes 3534852 | tf_op jit(solution)/shard_map/rt,rd->td/dot_general | solution.py:16
  145.4 2.9 %all_gather.3 = bf16[224,2048]{1,0:T(8,128)(2,1)S(1)} all-gather(bf16[224,1024]{1,0:T(8,128)(2,1)S(1)} %fusion.12), channel_id=1, replica_groups=mesh['sp'=16,'tp'=2] {'tp'}, dimensions={1}, use_global_device_ids=true | all-gather | bytes 1376256 | tf_op jit(solution)/shard_map/all_gather | solution.py:170
  152.0 1.7 reshape.201
  156.3 11.6 %all-to-all-start.2 = ((f32[16,8,513]{2,1,0:T(8,128)}), f32[16,8,513]{2,1,0:T(8,128)}, u32[]{:S(2)}, u32[]{:S(2)}) async-start(f32[16,8,513]{2,1,0:T(8,128)} %pad_maximum_fusion.3), calls=%async_computation.2 | async-start | bytes 655360 | tf_op jit(solution)/shard_map/all_to_all | solution.py:182
  167.9 1.7 fusion.75
  171.2 1.9 collective-permute-start.2
  176.4 1.5 collective-permute-start.6
  177.9 1.8 copy.175
  179.7 1.5 slice.38
  185.8 4.8 %all-to-all-start.3 = ((f32[16,8,512]{2,1,0:T(8,128)}), f32[16,8,512]{2,1,0:T(8,128)}, u32[]{:S(2)}, u32[]{:S(2)}) async-start(f32[16,8,512]{2,1,0:T(8,128)} %copy.166), calls=%async_computation.3 | async-start | bytes 524288 | tf_op jit(solution)/shard_map/all_to_all | solution.py:202
  190.7 1.7 bitcast_add_fusion.1
  192.4 1.9 collective-permute-start.3
  195.5 1.5 collective-permute-start.7
  197.1 4.9 %collective-permute-done.3 = bf16[2,2,128,256]{3,2,1,0:T(8,128)(2,1)S(1)} collective-permute-done((bf16[2,2,128,256]{3,2,1,0:T(8,128)(2,1)S(1)}, bf16[2,2,128,256]{3,2,1,0:T(8,128)(2,1)S(1)}, u32[]{:S(2)}, u32[]{:S(2)}) %collective-permute-start.3) | collective-permute-done | bytes 262176 | tf_op jit(solution)/shard_map/ppermute | solution.py:44
  202.0 1.6 collective-permute-start.4
  204.6 3.5 %collective-permute-done.4 = bf16[2,128,256]{2,1,0:T(8,128)(2,1)S(1)} collective-permute-done((bf16[2,128,256]{2,1,0:T(8,128)(2,1)S(1)}, bf16[2,128,256]{2,1,0:T(8,128)(2,1)S(1)}, u32[]{:S(2)}, u32[]{:S(2)}) %collective-permute-start.4) | collective-permute-done | bytes 131104 | tf_op jit(solution)/shard_map/ppermute | solution.py:44
  208.2 2.5 %collective-permute-start.5 = (bf16[128,256]{1,0:T(8,128)(2,1)S(1)}, bf16[128,256]{1,0:T(8,128)(2,1)S(1)}, u32[]{:S(2)}, u32[]{:S(2)}) collective-permute-start(bf16[128,256]{1,0:T(8,128)(2,1)S(1)} %fusion.57), channel_id=1, source_target_pairs={{0,16},{2,18},{4,20},{6,22},{8,24},{10,26},{12,28},{14,30},{16,0},... | collective-permute-start | bytes 196616 | tf_op jit(solution)/shard_map/ppermute | solution.py:44
  210.7 1.8 collective-permute-start.9
  213.6 3.0 %collective-permute-done.9 = bf16[128,256]{1,0:T(8,128)(2,1)S(1)} collective-permute-done((bf16[128,256]{1,0:T(8,128)(2,1)S(1)}, bf16[128,256]{1,0:T(8,128)(2,1)S(1)}, u32[]{:S(2)}, u32[]{:S(2)}) %collective-permute-start.9) | collective-permute-done | bytes 65568 | tf_op jit(solution)/shard_map/ppermute | solution.py:44
  219.1 1.6 convert_element_type.249
  220.8 2.0 convolution_bitcast_fusion.2
  222.8 2.1 fusion.26
  224.9 2.1 fusion.32
  233.4 1.8 copy.174
  (188 shorter events, 40.5 us)
Async XLA Ops:
  0.6 147.6 %copy-start = (bf16[2048,512]{1,0:T(8,128)(2,1)S(1)}, bf16[2048,512]{1,0:T(8,128)(2,1)}, u32[]{:S(2)}) copy-start(bf16[2048,512]{1,0:T(8,128)(2,1)} %param.27) | copy-start | bytes 6291460
  4.5 4.4 %copy-start.31 = (pred[1152,224]{0,1:T(8,128)(4,1)}, pred[1152,224]{0,1:T(8,128)(4,1)S(1)}, u32[]{:S(2)}) copy-start(pred[1152,224]{0,1:T(8,128)(4,1)S(1)} %fusion.11) | copy-start | bytes 774148
  8.9 8.7 %copy-start.42 = (f32[8,224]{1,0:T(8,128)S(1)}, f32[8,224]{1,0:T(8,128)}, u32[]{:S(2)}) copy-start(f32[8,224]{1,0:T(8,128)} %param.24) | copy-start | bytes 21508
  8.9 9.0 %copy-start.33 = (bf16[224,512]{1,0:T(8,128)(2,1)S(1)}, bf16[224,512]{1,0:T(8,128)(2,1)}, u32[]{:S(2)}) copy-start(bf16[224,512]{1,0:T(8,128)(2,1)} %param.21) | copy-start | bytes 688132
  8.9 9.4 %copy-start.34 = (bf16[224,512]{1,0:T(8,128)(2,1)S(1)}, bf16[224,512]{1,0:T(8,128)(2,1)}, u32[]{:S(2)}) copy-start(bf16[224,512]{1,0:T(8,128)(2,1)} %param.25) | copy-start | bytes 688132
  8.9 9.6 %copy-start.23 = (f32[1,8,64,128]{3,2,1,0:T(8,128)S(1)}, f32[1,8,64,128]{3,2,1,0:T(8,128)}, u32[]{:S(2)}) copy-start(f32[1,8,64,128]{3,2,1,0:T(8,128)} %param.26) | copy-start | bytes 786436
  8.9 56.1 %all-to-all-start = ((bf16[16,72,1024]{2,1,0:T(8,128)(2,1)}), bf16[16,72,1024]{2,1,0:T(8,128)(2,1)}, u32[]{:S(2)}, u32[]{:S(2)}) async-start(bf16[16,72,1024]{2,1,0:T(8,128)(2,1)} %bitcast.266), calls=%async_computation | async-start | bytes 4718592 | tf_op jit(solution)/shard_map/all_to_all | solution.py:89
  17.8 8.3 %copy-start.35 = (f32[8,224]{1,0:T(8,128)}, f32[8,224]{1,0:T(8,128)S(1)}, u32[]{:S(2)}) copy-start(f32[8,224]{1,0:T(8,128)S(1)} %convolution_bitcast_fusion.3) | copy-start | bytes 21508
  18.2 7.9 %copy-start.37 = (f32[8]{0:T(128)}, f32[8]{0:T(128)S(1)}, u32[]{:S(2)}) copy-start(f32[8]{0:T(128)S(1)} %slice_reduce_fusion.1) | copy-start | bytes 100
  29.2 14.5 %copy-start.5 = (bf16[16,72,2048]{2,1,0:T(8,128)(2,1)}, bf16[16,72,2048]{2,1,0:T(8,128)(2,1)S(1)}, u32[]{:S(2)}) copy-start(bf16[16,72,2048]{2,1,0:T(8,128)(2,1)S(1)} %pad.9) | copy-start | bytes 14155780
  31.9 5.8 %copy-start.15 = (f32[2,4,224,64]{2,3,1,0:T(8,128)}, f32[2,4,224,64]{2,3,1,0:T(8,128)S(1)}, u32[]{:S(2)}) copy-start(f32[2,4,224,64]{2,3,1,0:T(8,128)S(1)} %fusion.72) | copy-start | bytes 1376260
  45.1 20.0 %copy-start.22 = (bf16[512,1024]{1,0:T(8,128)(2,1)S(1)}, bf16[512,1024]{1,0:T(8,128)(2,1)}, u32[]{:S(2)}) copy-start(bf16[512,1024]{1,0:T(8,128)(2,1)} %get-tuple-element.34) | copy-start | bytes 3145732
  65.1 4.8 %copy-start.21 = (bf16[512,1024]{1,0:T(8,128)(2,1)S(1)}, bf16[512,1024]{1,0:T(8,128)(2,1)}, u32[]{:S(2)}) copy-start(bf16[512,1024]{1,0:T(8,128)(2,1)} %get-tuple-element.35) | copy-start | bytes 3145732
  65.1 4.8 %copy-start.44 = (f32[1152,512]{1,0:T(8,128)S(1)}, f32[1152,512]{1,0:T(8,128)}, u32[]{:S(2)}) copy-start(f32[1152,512]{1,0:T(8,128)} %copy-done.43) | copy-start | bytes 7077892
  65.1 4.8 %copy-start.45 = (f32[1152,512]{1,0:T(8,128)S(1)}, f32[1152,512]{1,0:T(8,128)}, u32[]{:S(2)}) copy-start(f32[1152,512]{1,0:T(8,128)} %get-tuple-element.36) | copy-start | bytes 7077892
  65.1 4.7 %collective-permute-start = (bf16[1152,1024]{1,0:T(8,128)(2,1)}, bf16[1152,1024]{1,0:T(8,128)(2,1)S(1)}, u32[]{:S(2)}, u32[]{:S(2)}) collective-permute-start(bf16[1152,1024]{1,0:T(8,128)(2,1)} %bitcast.4), channel_id=1, source_target_pairs={{0,1},{1,0},{2,3},{3,2},{4,5},{5,4},{6,7},{7,6},{8,9},{9,8},{10,11... | collective-permute-start | bytes 7077896 | tf_op jit(solution)/shard_map/ppermute | solution.py:21
  68.3 4.1 %copy-start.13 = (bf16[1024,1024]{1,0:T(8,128)(2,1)S(1)}, bf16[1024,1024]{1,0:T(8,128)(2,1)}, u32[]{:S(2)}) copy-start(bf16[1024,1024]{1,0:T(8,128)(2,1)} %get-tuple-element.39) | copy-start | bytes 6291460
  72.4 7.6 %copy-start.46 = (bf16[1152,512]{1,0:T(8,128)(2,1)}, bf16[1152,512]{1,0:T(8,128)(2,1)S(1)}, u32[]{:S(2)}) copy-start(bf16[1152,512]{1,0:T(8,128)(2,1)S(1)} %get-tuple-element.121) | copy-start | bytes 3538948
  72.4 7.5 %copy-start.48 = (bf16[1152,512]{1,0:T(8,128)(2,1)}, bf16[1152,512]{1,0:T(8,128)(2,1)S(1)}, u32[]{:S(2)}) copy-start(bf16[1152,512]{1,0:T(8,128)(2,1)S(1)} %get-tuple-element.122) | copy-start | bytes 3538948
  72.5 7.5 %copy-start.12 = (bf16[1024,1024]{1,0:T(8,128)(2,1)S(1)}, bf16[1024,1024]{1,0:T(8,128)(2,1)}, u32[]{:S(2)}) copy-start(bf16[1024,1024]{1,0:T(8,128)(2,1)} %get-tuple-element.38) | copy-start | bytes 6291460
  75.4 4.6 %collective-permute-start.1 = (bf16[1152,1024]{1,0:T(8,128)(2,1)S(1)}, bf16[1152,1024]{1,0:T(8,128)(2,1)S(1)}, u32[]{:S(2)}, u32[]{:S(2)}) collective-permute-start(bf16[1152,1024]{1,0:T(8,128)(2,1)S(1)} %convolution_convert_fusion), channel_id=1, source_target_pairs={{0,1},{1,0},{2,3},{3,2},{4,5},{5,4},{6,7},{7,6},{8,9},{9,8},{10,11... | collective-permute-start | bytes 7077896 | tf_op jit(solution)/shard_map/ppermute | solution.py:21
  84.0 19.0 %slice-start = ((s8[4718592]{0:T(1024)(128)(4,1)}), s8[524288]{0:T(1024)(128)(4,1)S(1)}, s32[]{:S(2)}) async-start(s8[4718592]{0:T(1024)(128)(4,1)} %bitcast.258), calls=%async_computation.4 | async-start | bytes 1048576
  84.0 59.0 %all-to-all-start.1 = ((bf16[16,72,1024]{2,1,0:T(8,128)(2,1)}), bf16[16,72,1024]{2,1,0:T(8,128)(2,1)}, u32[]{:S(2)}, u32[]{:S(2)}) async-start(bf16[16,72,1024]{2,1,0:T(8,128)(2,1)} %bitcast.265), calls=%async_computation.1 | async-start | bytes 4718592 | tf_op jit(solution)/shard_map/all_to_all | solution.py:154
  95.9 7.1 %slice-start.1 = ((s8[4718592]{0:T(1024)(128)(4,1)}), s8[4194304]{0:T(1024)(128)(4,1)S(1)}, s32[]{:S(2)}) async-start(s8[4718592]{0:T(1024)(128)(4,1)} %bitcast.258), calls=%async_computation.5 | async-start | bytes 8388608
  95.9 7.1 %copy-start.47 = (bf16[1152,512]{1,0:T(8,128)(2,1)S(1)}, bf16[1152,512]{1,0:T(8,128)(2,1)}, u32[]{:S(2)}) copy-start(bf16[1152,512]{1,0:T(8,128)(2,1)} %copy-done.46) | copy-start | bytes 3538948
  103.0 4.2 %copy-start.40 = (bf16[1152,1024]{1,0:T(8,128)(2,1)S(1)}, bf16[1152,1024]{1,0:T(8,128)(2,1)}, u32[]{:S(2)}) copy-start(bf16[1152,1024]{1,0:T(8,128)(2,1)} %copy-done.39) | copy-start | bytes 7077892
  103.0 4.1 %copy-start.49 = (bf16[1152,512]{1,0:T(8,128)(2,1)S(1)}, bf16[1152,512]{1,0:T(8,128)(2,1)}, u32[]{:S(2)}) copy-start(bf16[1152,512]{1,0:T(8,128)(2,1)} %get-tuple-element.40) | copy-start | bytes 3538948
  107.1 35.8 %copy-start.32 = (pred[1152,224]{0,1:T(8,128)(4,1)S(1)}, pred[1152,224]{0,1:T(8,128)(4,1)}, u32[]{:S(2)}) copy-start(pred[1152,224]{0,1:T(8,128)(4,1)} %copy-done.31) | copy-start | bytes 774148
  107.1 35.8 %copy-start.41 = (bf16[224,2048]{1,0:T(8,128)(2,1)S(1)}, bf16[224,2048]{1,0:T(8,128)(2,1)}, u32[]{:S(2)}) copy-start(bf16[224,2048]{1,0:T(8,128)(2,1)} %param.14) | copy-start | bytes 2752516
  145.4 3.8 %copy-start.7 = (f32[2,4,224,64]{2,3,1,0:T(8,128)S(1)}, f32[2,4,224,64]{2,3,1,0:T(8,128)}, u32[]{:S(2)}) copy-start(f32[2,4,224,64]{2,3,1,0:T(8,128)} %get-tuple-element.47) | copy-start | bytes 1376260
  156.3 23.3 %all-to-all-start.2 = ((f32[16,8,513]{2,1,0:T(8,128)}), f32[16,8,513]{2,1,0:T(8,128)}, u32[]{:S(2)}, u32[]{:S(2)}) async-start(f32[16,8,513]{2,1,0:T(8,128)} %pad_maximum_fusion.3), calls=%async_computation.2 | async-start | bytes 655360 | tf_op jit(solution)/shard_map/all_to_all | solution.py:182
  170.2 4.7 %copy-start.4 = (f32[16,128,256]{2,1,0:T(8,128)}, f32[16,128,256]{2,1,0:T(8,128)S(1)}, u32[]{:S(2)}) copy-start(f32[16,128,256]{2,1,0:T(8,128)S(1)} %get-tuple-element.123) | copy-start | bytes 6291460
  170.2 4.7 %copy-start.2 = (f32[16,128,256]{2,1,0:T(8,128)}, f32[16,128,256]{2,1,0:T(8,128)S(1)}, u32[]{:S(2)}) copy-start(f32[16,128,256]{2,1,0:T(8,128)S(1)} %get-tuple-element.124) | copy-start | bytes 6291460
  171.2 19.5 %collective-permute-start.2 = (bf16[2,2,2,128,256]{4,3,2,1,0:T(8,128)(2,1)}, bf16[2,2,2,128,256]{4,3,2,1,0:T(8,128)(2,1)}, u32[]{:S(2)}, u32[]{:S(2)}) collective-permute-start(bf16[2,2,2,128,256]{4,3,2,1,0:T(8,128)(2,1)} %fusion.23), channel_id=1, source_target_pairs={{0,2},{2,0},{4,6},{6,4},{8,10},{10,8},{12,14},{14,12},{16,18},{18,... | collective-permute-start | bytes 1572872 | tf_op jit(solution)/shard_map/ppermute | solution.py:44
  173.6 9.5 %copy-start.38 = (pred[16,16]{1,0:T(8,128)(4,1)S(1)}, pred[16,16]{1,0:T(8,128)(4,1)}, u32[]{:S(2)}) copy-start(pred[16,16]{1,0:T(8,128)(4,1)} %get-tuple-element.143) | copy-start | bytes 772
  176.4 17.9 %collective-permute-start.6 = (bf16[2,2,2,128,256]{4,3,0,1,2:T(8,128)(2,1)}, bf16[2,2,2,128,256]{4,3,0,1,2:T(8,128)(2,1)}, u32[]{:S(2)}, u32[]{:S(2)}) collective-permute-start(bf16[2,2,2,128,256]{4,3,0,1,2:T(8,128)(2,1)} %fusion.24), channel_id=1, source_target_pairs={{0,4},{2,6},{4,0},{6,2},{8,12},{10,14},{12,8},{14,10},{16,20},{18,... | collective-permute-start | bytes 1572872 | tf_op jit(solution)/shard_map/ppermute | solution.py:44
  185.8 31.6 %all-to-all-start.3 = ((f32[16,8,512]{2,1,0:T(8,128)}), f32[16,8,512]{2,1,0:T(8,128)}, u32[]{:S(2)}, u32[]{:S(2)}) async-start(f32[16,8,512]{2,1,0:T(8,128)} %copy.166), calls=%async_computation.3 | async-start | bytes 524288 | tf_op jit(solution)/shard_map/all_to_all | solution.py:202
  192.4 9.6 %collective-permute-start.3 = (bf16[2,2,128,256]{3,2,1,0:T(8,128)(2,1)S(1)}, bf16[2,2,128,256]{3,2,1,0:T(8,128)(2,1)S(1)}, u32[]{:S(2)}, u32[]{:S(2)}) collective-permute-start(bf16[2,2,128,256]{3,2,1,0:T(8,128)(2,1)S(1)} %fusion.34), channel_id=1, source_target_pairs={{0,4},{2,6},{4,0},{6,2},{8,12},{10,14},{12,8},{14,10},{16,20},{18,... | collective-permute-start | bytes 786440 | tf_op jit(solution)/shard_map/ppermute | solution.py:44
  195.5 8.1 %collective-permute-start.7 = (bf16[2,2,128,256]{3,2,0,1:T(8,128)(2,1)S(1)}, bf16[2,2,128,256]{3,2,0,1:T(8,128)(2,1)S(1)}, u32[]{:S(2)}, u32[]{:S(2)}) collective-permute-start(bf16[2,2,128,256]{3,2,0,1:T(8,128)(2,1)S(1)} %fusion.35), channel_id=1, source_target_pairs={{0,2},{2,0},{4,6},{6,4},{8,10},{10,8},{12,14},{14,12},{16,18},{18,... | collective-permute-start | bytes 786440 | tf_op jit(solution)/shard_map/ppermute | solution.py:44
  202.0 6.1 %collective-permute-start.4 = (bf16[2,128,256]{2,1,0:T(8,128)(2,1)S(1)}, bf16[2,128,256]{2,1,0:T(8,128)(2,1)S(1)}, u32[]{:S(2)}, u32[]{:S(2)}) collective-permute-start(bf16[2,128,256]{2,1,0:T(8,128)(2,1)S(1)} %fusion.42), channel_id=1, source_target_pairs={{0,8},{2,10},{4,12},{6,14},{8,0},{10,2},{12,4},{14,6},{16,24},{18,... | collective-permute-start | bytes 393224 | tf_op jit(solution)/shard_map/ppermute | solution.py:44
  203.7 7.0 %collective-permute-start.8 = (bf16[2,128,256]{2,1,0:T(8,128)(2,1)S(1)}, bf16[2,128,256]{2,1,0:T(8,128)(2,1)S(1)}, u32[]{:S(2)}, u32[]{:S(2)}) collective-permute-start(bf16[2,128,256]{2,1,0:T(8,128)(2,1)S(1)} %fusion.43), channel_id=1, source_target_pairs={{0,8},{2,10},{4,12},{6,14},{8,0},{10,2},{12,4},{14,6},{16,24},{18,... | collective-permute-start | bytes 393224 | tf_op jit(solution)/shard_map/ppermute | solution.py:44
  208.2 5.4 %collective-permute-start.5 = (bf16[128,256]{1,0:T(8,128)(2,1)S(1)}, bf16[128,256]{1,0:T(8,128)(2,1)S(1)}, u32[]{:S(2)}, u32[]{:S(2)}) collective-permute-start(bf16[128,256]{1,0:T(8,128)(2,1)S(1)} %fusion.57), channel_id=1, source_target_pairs={{0,16},{2,18},{4,20},{6,22},{8,24},{10,26},{12,28},{14,30},{16,0},... | collective-permute-start | bytes 196616 | tf_op jit(solution)/shard_map/ppermute | solution.py:44
  210.7 5.9 %collective-permute-start.9 = (bf16[128,256]{1,0:T(8,128)(2,1)S(1)}, bf16[128,256]{1,0:T(8,128)(2,1)S(1)}, u32[]{:S(2)}, u32[]{:S(2)}) collective-permute-start(bf16[128,256]{1,0:T(8,128)(2,1)S(1)} %fusion.58), channel_id=1, source_target_pairs={{0,16},{2,18},{4,20},{6,22},{8,24},{10,26},{12,28},{14,30},{16,0},... | collective-permute-start | bytes 196616 | tf_op jit(solution)/shard_map/ppermute | solution.py:44
  220.7 4.1 %copy-start.6 = (f32[2,4,224,64]{2,3,1,0:T(8,128)S(1)}, f32[2,4,224,64]{2,3,1,0:T(8,128)}, u32[]{:S(2)}) copy-start(f32[2,4,224,64]{2,3,1,0:T(8,128)} %fusion.77) | copy-start | bytes 1376260
  220.7 4.1 %copy-start.8 = (f32[2,4,224,64]{2,3,1,0:T(8,128)S(1)}, f32[2,4,224,64]{2,3,1,0:T(8,128)}, u32[]{:S(2)}) copy-start(f32[2,4,224,64]{2,3,1,0:T(8,128)} %get-tuple-element.47) | copy-start | bytes 1376260
  220.7 4.2 %copy-start.16 = (f32[2,4,224,64]{2,3,1,0:T(8,128)S(1)}, f32[2,4,224,64]{2,3,1,0:T(8,128)}, u32[]{:S(2)}) copy-start(f32[2,4,224,64]{2,3,1,0:T(8,128)} %copy-done.15) | copy-start | bytes 1376260
  220.7 4.2 %copy-start.17 = (f32[2,4,224,64]{2,3,1,0:T(8,128)S(1)}, f32[2,4,224,64]{2,3,1,0:T(8,128)}, u32[]{:S(2)}) copy-start(f32[2,4,224,64]{2,3,1,0:T(8,128)} %get-tuple-element.54) | copy-start | bytes 1376260
  227.0 8.2 %copy-start.36 = (f32[8,224]{1,0:T(8,128)S(1)}, f32[8,224]{1,0:T(8,128)}, u32[]{:S(2)}) copy-start(f32[8,224]{1,0:T(8,128)} %copy-done.35) | copy-start | bytes 21508
  (18 other events, 47.6 us)
